TPU v7x, 32 devices: a whole 2x2x4 slice. The times are simulated.
32 devices in a mesh: gr: 2 (over x), sp: 8 (over z, y), tp: 2 (over core).
Axes of the slice: x: 2, y: 2, z: 4, core: 2. Of those that a mesh axis runs over, the one named last changes fastest.
Arguments:
- tokens: bfloat16 [8, 1536, 2048], P('gr', 'sp'), parts along dimension 0, may hold values from -6 to 6
- key_weight: bfloat16 [2048, 512], P(None, 'tp'), may hold values from -0.125 to 0.125
- value_weight: bfloat16 [2048, 1024], P(None, 'tp'), may hold values from -0.125 to 0.125
- input_weight: bfloat16 [2048, 8], P(None, 'tp'), may hold values from -0.125 to 0.125
- forget_weight: bfloat16 [2048, 8], P(None, 'tp'), may hold values from -0.125 to 0.125
- forget_bias: float32 [8], P('tp'), may hold values from 2.5 to 9.5
- query: bfloat16 [8, 512], P('gr', 'tp'), parts along dimension 0, may hold values from -6 to 6
Outputs:
- key_cache: bfloat16 [16, 768, 512], P(('gr', 'sp'), None, 'tp'), parts along dimension 0
- value_cache: bfloat16 [16, 768, 1024], P(('gr', 'sp'), None, 'tp'), parts along dimension 0
- memory: float32 [8, 8, 64, 128], P('gr', 'tp'), parts along dimension 0
- normalizer: float32 [8, 8, 64], P('gr', 'tp'), parts along dimension 0
- stabilizer: float32 [8, 8], P('gr', 'tp'), parts along dimension 0
- first_read: float32 [8, 1024], P('gr', 'tp'), parts along dimension 0
There are 2 independent parts, one for each index of `gr`. A program takes and returns all parts, laid end to end along the dimension named above; an argument that names none is the same for every part. Nothing has to cross between parts.
All inputs are finite; a program needn't handle non-finite values.
Results may differ from a plain program's by a relative error of at most 0.0015.
The roundings to bfloat16 on the way count: a program that leaves them out, or rounds other values in their place, can miss the bound.
Values may be sent and summed in bfloat16 or wider, within the bound.
A program may use at most 64 MiB of HBM per device.

v0:
```python
import jax
import jax.numpy as jnp
from jax import lax
from jax.sharding import PartitionSpec as P


def carried_in(array, axis, combine, identity):
    size, index = (lax.axis_size(axis), lax.axis_index(axis))
    everything = lax.all_gather(array, axis)
    start = jnp.broadcast_to(jnp.asarray(identity, array.dtype), array.shape)

    def step(k, before):
        at = size - 1 - k
        reached = at > index
        new = combine(before, everything[at])
        return jnp.where(reached, new, before)

    return lax.fori_loop(0, size, step, start)


def merged(value, axis, join):
    pieces = jax.tree.map(lambda part: lax.all_gather(part, axis), value)
    head = jax.tree.map(lambda part: part[0], pieces)
    tail = jax.tree.map(lambda part: part[1:], pieces)
    so_far, _ = lax.scan(lambda so_far, share: (join(so_far, share), None), head, tail)
    return so_far


def add_pair(earlier, later):
    return earlier + later


def block_state(keys3, values3, igate, logf, later, kdim):
    seqs, span, heads = logf.shape
    total = jnp.sum(logf, axis=1)
    logw = (later + total)[:, None, :] - jnp.cumsum(logf, axis=1) + igate
    top = jnp.max(logw, axis=1)
    weight = jnp.exp(logw - top[:, None, :]) * kdim ** (-0.5)
    keys4 = keys3.reshape(seqs, span, heads, kdim).astype(jnp.float32)
    values4 = values3.reshape(seqs, span, heads, -1).astype(jnp.float32)
    scaled = keys4 * weight[..., None]
    memory = jnp.einsum("slhd,slhe->shde", scaled, values4, precision=lax.Precision.HIGHEST)
    return (memory, jnp.sum(scaled, axis=1), top, total)


def merge_states(first, second):
    top = jnp.maximum(first[2], second[2])
    left = jnp.exp(first[2] - top)
    right = jnp.exp(second[2] - top)
    memory = first[0] * left[..., None, None] + second[0] * right[..., None, None]
    normal = first[1] * left[..., None] + second[1] * right[..., None]
    return (memory, normal, top, first[3] + second[3])


def local(tokens, key_weight, value_weight, input_weight, forget_weight, forget_bias, query):
    seqs, span, width = tokens.shape
    heads = input_weight.shape[1]
    kdim = key_weight.shape[1] // heads
    vdim = value_weight.shape[1] // heads
    pieces = lax.axis_size("sp") // seqs
    sub = span // pieces
    flat = tokens.reshape(seqs * span, width)
    keys = jnp.dot(flat, key_weight, preferred_element_type=jnp.float32).astype(jnp.bfloat16)
    values = jnp.dot(flat, value_weight, preferred_element_type=jnp.float32).astype(jnp.bfloat16)
    gate_pair = jnp.concatenate([input_weight, forget_weight], axis=1)
    gates = jnp.dot(flat, gate_pair, preferred_element_type=jnp.float32)
    igate = gates[:, :heads].reshape(seqs, span, heads)
    logf = jax.nn.log_sigmoid(gates[:, heads:] + forget_bias).reshape(seqs, span, heads)
    keys3 = keys.reshape(seqs, span, heads * kdim)
    values3 = values.reshape(seqs, span, heads * vdim)
    key_cache, value_cache = (
        lax.all_to_all(
            keys3.reshape(seqs * pieces, sub, heads * kdim),
            "sp",
            split_axis=0,
            concat_axis=1,
            tiled=True,
        ),
        lax.all_to_all(
            values3.reshape(seqs * pieces, sub, heads * vdim),
            "sp",
            split_axis=0,
            concat_axis=1,
            tiled=True,
        ),
    )
    zeros = jnp.zeros((seqs, heads), jnp.float32)
    later = carried_in(jnp.sum(logf, axis=1), "sp", add_pair, zeros)
    memory_part, normal_part, top, total = block_state(keys3, values3, igate, logf, later, kdim)
    memory_all, normal_all, top_all, total_all = merged(
        (memory_part, normal_part, top, total), "sp", merge_states
    )
    stabilizer = jnp.maximum(top_all, total_all)
    factor = jnp.exp(top_all - stabilizer)
    memory = memory_all * factor[..., None, None]
    normalizer = normal_all * factor[..., None]
    asked = query.astype(jnp.float32).reshape(query.shape[0], heads, kdim)
    numer = jnp.einsum("shd,shde->she", asked, memory, precision=lax.Precision.HIGHEST)
    denom = jnp.maximum(jnp.abs(jnp.sum(asked * normalizer, axis=-1)), 1.0)
    first_read = (numer / denom[..., None]).reshape(query.shape[0], heads * vdim)
    return (key_cache, value_cache, memory, normalizer, stabilizer, first_read)


def solution(mesh):
    return jax.shard_map(
        local,
        mesh=mesh,
        in_specs=(
            P("gr", "sp", None),
            P(None, "tp"),
            P(None, "tp"),
            P(None, "tp"),
            P(None, "tp"),
            P("tp"),
            P("gr", "tp"),
        ),
        out_specs=(
            P(("gr", "sp"), None, "tp"),
            P(("gr", "sp"), None, "tp"),
            P("gr", "tp", None, None),
            P("gr", "tp", None),
            P("gr", "tp"),
            P("gr", "tp"),
        ),
        check_vma=False,
    )
```

profile of v0, /device:TPU:0, one launch (start us, length us, event | category | flops | bytes accessed | tf_op | source)
XLA Modules:
  0.0 211.6 jit_solution(7671632423110484531)
XLA Ops:
  7.2 1.8 copy-done
  9.1 2.4 %convolution_convert_fusion.1 = bf16[768,256]{1,0:T(8,128)(2,1)S(1)} fusion(bf16[768,2048]{1,0:T(8,128)(2,1)S(1)} %bitcast.70, bf16[2048,256]{1,0:T(8,128)(2,1)} %param.12), kind=kOutput, calls=%fused_computation.11 | convolution fusion | flops 805502976 | bytes 4587520 | tf_op jit(solution)/shard_map/dot_general | solution.py:63
  11.4 2.7 %convolution_convert_fusion = bf16[768,512]{1,0:T(8,128)(2,1)} fusion(bf16[768,2048]{1,0:T(8,128)(2,1)S(1)} %bitcast.71, bf16[2048,512]{1,0:T(8,128)(2,1)S(1)} %copy-done.6), kind=kOutput, calls=%fused_computation.10 | convolution fusion | flops 1611005952 | bytes 6029312 | tf_op jit(solution)/shard_map/dot_general | solution.py:64
  14.1 1.1 copy.31
  15.2 2.8 %reshape.70 = f32[4,192,4,64]{1,0,3,2:T(4,128)} reshape(f32[768,256]{0,1:T(8,128)} %copy.31) | data formatting | bytes 1572864 | tf_op jit(solution)/shard_map/convert_element_type | solution.py:39
  18.1 1.6 convolution_bitcast_fusion
  20.1 4.8 %reduce-window.6 = f32[4,4,2,128]{3,2,1,0:T(2,128)S(1)} reduce-window(f32[4,4,2,128]{3,2,1,0:T(2,128)S(1)} %copy.34, f32[]{:T(128)} %constant.71.clone.1), window={size=1x1x1x128 pad=0_0x0_0x0_0x127_0}, to_apply=%region_3.4 | reduce-window | flops 520192 | bytes 32772 | tf_op jit(solution)/shard_map/reduce-window
  25.1 0.1 copy.35
  25.2 0.1 copy.36
  25.6 27.9 %all-gather.4 = f32[8,4,4]{2,1,0:T(4,128)S(1)} all-gather(f32[1,4,4]{2,1,0:T(4,128)S(1)} %bitcast.83), channel_id=2, replica_groups=mesh['gr'=2,'sp'=8,'tp'=2] {'sp'}, dimensions={0}, use_global_device_ids=true | all-gather | bytes 576 | tf_op jit(solution)/shard_map/all_gather | solution.py:9
  53.5 0.3 while.33
  53.9 0.2 fusion.14
  54.2 2.4 %reshape_reshape.12 = bf16[4,192,4,128]{3,2,1,0:T(4,128)(2,1)} reshape(bf16[768,512]{1,0:T(8,128)(2,1)} %convolution_convert_fusion) | data formatting | bytes 1572864 | tf_op jit(solution)/shard_map/reshape;reshape | solution.py:40
  56.6 2.3 %fusion.16 = (f32[4,4,64]{0,2,1:T(8,128)}, f32[4,192,4,64]{1,0,3,2:T(4,128)S(1)}) fusion(f32[4,192,4,64]{1,0,3,2:T(4,128)} %reshape.70, f32[4,192,4]{1,0,2:T(4,128)S(1)} %exponential_multiply_fusion), kind=kLoop, calls=%fused_computation.42 | loop fusion | flops 392192 | bytes 1589248 | tf_op jit(solution)/shard_map/reduce_sum | solution.py:43
  58.9 2.9 %fusion.3 = f32[4,4,64,128]{3,2,1,0:T(8,128)} fusion(f32[4,192,4,64]{1,0,3,2:T(4,128)S(1)} %get-tuple-element.219, bf16[4,192,4,128]{3,2,1,0:T(4,128)(2,1)} %reshape_reshape.12), kind=kOutput, calls=%fused_computation.13 | convolution fusion | flops 301989888 | bytes 2097152 | tf_op jit(solution)/shard_map/slhd,slhe->shde/dot_general | solution.py:42
  61.8 15.3 %all_to_all.24 = bf16[8,96,256]{2,1,0:T(8,128)(2,1)S(1)} all-to-all(bf16[8,96,256]{2,1,0:T(8,128)(2,1)} %bitcast.76), channel_id=1, replica_groups=mesh['gr'=2,'sp'=8,'tp'=2] {'sp'}, dimensions={0} | all-to-all | bytes 786432 | tf_op jit(solution)/shard_map/all_to_all | solution.py:72
  77.2 10.2 %all-to-all-start.1 = ((bf16[8,96,512]{2,1,0:T(8,128)(2,1)}), bf16[8,96,512]{2,1,0:T(8,128)(2,1)}, u32[]{:S(2)}, u32[]{:S(2)}) async-start(bf16[8,96,512]{2,1,0:T(8,128)(2,1)} %bitcast.74), calls=%async_computation.1 | async-start | bytes 1572864 | tf_op jit(solution)/shard_map/all_to_all | solution.py:79
  87.4 1.0 copy.40
  88.4 41.4 %all-gather.2 = f32[32,4,64]{2,1,0:T(4,128)S(1)} all-gather(f32[4,4,64]{2,1,0:T(4,128)S(1)} %copy.40), channel_id=4, replica_groups=mesh['gr'=2,'sp'=8,'tp'=2] {'sp'}, dimensions={0}, use_global_device_ids=true | all-gather | bytes 36864 | tf_op jit(solution)/shard_map/all_gather | solution.py:22
  129.8 0.6 slice.75
  130.4 1.3 slice.76
  131.7 0.7 reshape.67
  132.4 0.7 reshape.101
  133.1 26.5 %all-gather.5 = f32[8,4,4]{2,1,0:T(4,128)S(1)} all-gather(f32[1,4,4]{2,1,0:T(4,128)S(1)} %bitcast.82), channel_id=5, replica_groups=mesh['gr'=2,'sp'=8,'tp'=2] {'sp'}, dimensions={0}, use_global_device_ids=true | all-gather | bytes 576 | tf_op jit(solution)/shard_map/all_gather | solution.py:22
  159.6 0.6 slice.73
  160.2 0.7 slice_bitcast_fusion
  160.9 1.9 slice.69
  162.8 4.4 %slice.74 = f32[28,4,64,128]{3,2,1,0:T(8,128)} slice(f32[32,4,64,128]{3,2,1,0:T(8,128)} %all-gather.8.cloned.1.call-done), slice={[4:32], [0:4], [0:64], [0:128]} | slice | bytes 7340032 | tf_op jit(solution)/shard_map/slice | solution.py:24
  167.1 30.0 %while.32 = (s32[]{:T(128)}, f32[4,4,64,128]{3,2,1,0:T(8,128)}, f32[4,4,64]{2,1,0:T(4,128)S(1)}, f32[4,4]{1,0:T(4,128)S(1)}, f32[4,4]{1,0:T(4,128)S(1)}, /*index...) while((s32[]{:T(128)}, f32[4,4,64,128]{3,2,1,0:T(8,128)}, ...), condition=%wide.region_8.9_spmd, body=%wide.region_7.8_spmd.sunk | while | flops 396354 | bytes 1586173 | solution.py:25
  167.1 0.7 subtract_exponential_fusion.3
  167.8 0.7 bitcast_add_fusion.2
  168.5 2.1 %fusion.27 = f32[4,4,64,128]{3,2,1,0:T(8,128)} fusion(f32[7,4,4,64,128]{4,3,2,1,0:T(8,128)} %get-tuple-element.362, s32[]{:T(128)S(6)} %copy.64, f32[4,4,64,128]{3,2,1,0:T(8,128)} %get-tuple-element.347, f32[4,4]{1,0:T(4,128)S(1)} %get-tuple-element.305, f32[4,4]{1,0:T(4,128)S(1)} %get-tuple-element.306), kind=kLoop, calls=%fused_computation.1.clone.1 | loop fusion | flops 393216 | bytes 1572996 | tf_op jit(solution)/shard_map/while/body/eval_jaxpr/add | solution.py:50
  170.6 0.8 fusion.28
  171.4 0.7 subtract_exponential_fusion.3
  172.1 0.7 bitcast_add_fusion.2
  172.8 2.1 %fusion.27 = f32[4,4,64,128]{3,2,1,0:T(8,128)} fusion(f32[7,4,4,64,128]{4,3,2,1,0:T(8,128)} %get-tuple-element.362, s32[]{:T(128)S(6)} %copy.64, f32[4,4,64,128]{3,2,1,0:T(8,128)} %get-tuple-element.347, f32[4,4]{1,0:T(4,128)S(1)} %get-tuple-element.305, f32[4,4]{1,0:T(4,128)S(1)} %get-tuple-element.306), kind=kLoop, calls=%fused_computation.1.clone.1 | loop fusion | flops 393216 | bytes 1572996 | tf_op jit(solution)/shard_map/while/body/eval_jaxpr/add | solution.py:50
  174.9 0.8 fusion.28
  175.7 0.7 subtract_exponential_fusion.3
  176.4 0.7 bitcast_add_fusion.2
  177.1 2.1 %fusion.27 = f32[4,4,64,128]{3,2,1,0:T(8,128)} fusion(f32[7,4,4,64,128]{4,3,2,1,0:T(8,128)} %get-tuple-element.362, s32[]{:T(128)S(6)} %copy.64, f32[4,4,64,128]{3,2,1,0:T(8,128)} %get-tuple-element.347, f32[4,4]{1,0:T(4,128)S(1)} %get-tuple-element.305, f32[4,4]{1,0:T(4,128)S(1)} %get-tuple-element.306), kind=kLoop, calls=%fused_computation.1.clone.1 | loop fusion | flops 393216 | bytes 1572996 | tf_op jit(solution)/shard_map/while/body/eval_jaxpr/add | solution.py:50
  179.2 0.8 fusion.28
  180.0 0.7 subtract_exponential_fusion.3
  180.7 0.7 bitcast_add_fusion.2
  181.4 2.1 %fusion.27 = f32[4,4,64,128]{3,2,1,0:T(8,128)} fusion(f32[7,4,4,64,128]{4,3,2,1,0:T(8,128)} %get-tuple-element.362, s32[]{:T(128)S(6)} %copy.64, f32[4,4,64,128]{3,2,1,0:T(8,128)} %get-tuple-element.347, f32[4,4]{1,0:T(4,128)S(1)} %get-tuple-element.305, f32[4,4]{1,0:T(4,128)S(1)} %get-tuple-element.306), kind=kLoop, calls=%fused_computation.1.clone.1 | loop fusion | flops 393216 | bytes 1572996 | tf_op jit(solution)/shard_map/while/body/eval_jaxpr/add | solution.py:50
  183.5 0.8 fusion.28
  184.3 0.7 subtract_exponential_fusion.3
  185.0 0.7 bitcast_add_fusion.2
  185.7 2.1 %fusion.27 = f32[4,4,64,128]{3,2,1,0:T(8,128)} fusion(f32[7,4,4,64,128]{4,3,2,1,0:T(8,128)} %get-tuple-element.362, s32[]{:T(128)S(6)} %copy.64, f32[4,4,64,128]{3,2,1,0:T(8,128)} %get-tuple-element.347, f32[4,4]{1,0:T(4,128)S(1)} %get-tuple-element.305, f32[4,4]{1,0:T(4,128)S(1)} %get-tuple-element.306), kind=kLoop, calls=%fused_computation.1.clone.1 | loop fusion | flops 393216 | bytes 1572996 | tf_op jit(solution)/shard_map/while/body/eval_jaxpr/add | solution.py:50
  187.8 0.8 fusion.28
  188.6 0.7 subtract_exponential_fusion.3
  189.3 0.7 bitcast_add_fusion.2
  189.9 2.1 %fusion.27 = f32[4,4,64,128]{3,2,1,0:T(8,128)} fusion(f32[7,4,4,64,128]{4,3,2,1,0:T(8,128)} %get-tuple-element.362, s32[]{:T(128)S(6)} %copy.64, f32[4,4,64,128]{3,2,1,0:T(8,128)} %get-tuple-element.347, f32[4,4]{1,0:T(4,128)S(1)} %get-tuple-element.305, f32[4,4]{1,0:T(4,128)S(1)} %get-tuple-element.306), kind=kLoop, calls=%fused_computation.1.clone.1 | loop fusion | flops 393216 | bytes 1572996 | tf_op jit(solution)/shard_map/while/body/eval_jaxpr/add | solution.py:50
  192.1 0.8 fusion.28
  192.8 0.7 subtract_exponential_fusion.3
  193.5 0.7 bitcast_add_fusion.2
  194.2 2.1 %fusion.27 = f32[4,4,64,128]{3,2,1,0:T(8,128)} fusion(f32[7,4,4,64,128]{4,3,2,1,0:T(8,128)} %get-tuple-element.362, s32[]{:T(128)S(6)} %copy.64, f32[4,4,64,128]{3,2,1,0:T(8,128)} %get-tuple-element.347, f32[4,4]{1,0:T(4,128)S(1)} %get-tuple-element.305, f32[4,4]{1,0:T(4,128)S(1)} %get-tuple-element.306), kind=kLoop, calls=%fused_computation.1.clone.1 | loop fusion | flops 393216 | bytes 1572996 | tf_op jit(solution)/shard_map/while/body/eval_jaxpr/add | solution.py:50
  196.3 0.8 fusion.28
  197.1 0.6 subtract_exponential_fusion.1
  197.7 1.1 broadcast_multiply_fusion.1
  198.9 1.3 multiply_reduce_fusion
  200.2 1.0 fusion.17
  201.4 0.6 copy.52
  202.0 0.7 copy.78
  202.7 2.1 copy.79
  (48 shorter events, 1.3 us)
Async XLA Ops:
  7.2 1.9 copy-start
  7.2 153.7 %all-gather.8.cloned.1.call-start = ((), (), s32[]{:S(2)}) async-start(), calls=%async_computation.2 | async-start | bytes 4718592 | tf_op jit(solution)/shard_map/all_gather | solution.py:22
  9.1 2.4 %copy-start.6 = (bf16[2048,512]{1,0:T(8,128)(2,1)S(1)}, bf16[2048,512]{1,0:T(8,128)(2,1)}, u32[]{:S(2)}) copy-start(bf16[2048,512]{1,0:T(8,128)(2,1)} %param.13) | copy-start | bytes 6291460
  11.4 2.7 %copy-start.2 = (bf16[768,256]{1,0:T(8,128)(2,1)}, bf16[768,256]{1,0:T(8,128)(2,1)S(1)}, u32[]{:S(2)}) copy-start(bf16[768,256]{1,0:T(8,128)(2,1)S(1)} %convolution_convert_fusion.1) | copy-start | bytes 1179652
  14.1 5.6 %copy-start.5 = (f32[4]{0:T(128)S(1)}, f32[4]{0:T(128)}, u32[]{:S(2)}) copy-start(f32[4]{0:T(128)} %param.16) | copy-start | bytes 52
  53.8 8.0 %copy-start.3 = (f32[8,4,4]{2,1,0:T(4,128)}, f32[8,4,4]{2,1,0:T(4,128)S(1)}, u32[]{:S(2)}) copy-start(f32[8,4,4]{2,1,0:T(4,128)S(1)} %get-tuple-element.384) | copy-start | bytes 1540
  58.9 72.8 %copy-start.4 = (bf16[4,256]{1,0:T(4,128)(2,1)S(1)}, bf16[4,256]{1,0:T(4,128)(2,1)}, u32[]{:S(2)}) copy-start(bf16[4,256]{1,0:T(4,128)(2,1)} %param.17) | copy-start | bytes 6148
  77.2 83.7 %all-to-all-start.1 = ((bf16[8,96,512]{2,1,0:T(8,128)(2,1)}), bf16[8,96,512]{2,1,0:T(8,128)(2,1)}, u32[]{:S(2)}, u32[]{:S(2)}) async-start(bf16[8,96,512]{2,1,0:T(8,128)(2,1)} %bitcast.74), calls=%async_computation.1 | async-start | bytes 1572864 | tf_op jit(solution)/shard_map/all_to_all | solution.py:79
  198.9 5.9 %copy-start.1 = (f32[4,4,64,128]{3,2,1,0:T(8,128)}, f32[4,4,64,128]{3,2,1,0:T(8,128)S(1)}, u32[]{:S(2)}) copy-start(f32[4,4,64,128]{3,2,1,0:T(8,128)S(1)} %broadcast_multiply_fusion.1) | copy-start | bytes 1572868
Sparse Core Ops, SparseCore 0:
  61.9 87.9 all-gather.7
where the time goes:
time: 213 us; the launch traced here: 212 us
  blocking collectives  111 us (52%)
  other arithmetic  40.9 us (19%)
  local copies, waits for them, and re-layouts  24.3 us (11%)
  between operations  14.2 us (7%)
  matrix products  10.6 us (5%)
  starting transfers between devices  10.2 us (5%)
    all_gather x2, blocking collectives, merged(): pieces = jax.tree.map(lambda part: lax.all_gather(part, axis), value)  67.9 us
    all_gather x1, blocking collectives, carried_in(): everything = lax.all_gather(array, axis)  27.9 us
    all_to_all x1, blocking collectives, local(): lax.all_to_all(keys3.reshape(seqs * pieces, sub, heads * kdim), 'sp', spl...  15.3 us
    add x7, other arithmetic, merge_states(): first[0] * left[..., None, None] + second[0] * right[..., None, None]  14.8 us
    all_to_all x1, starting transfers between devices, local(): lax.all_to_all(values3.reshape(seqs * pieces, sub, heads * vdim), 'sp', s...  10.2 us
    slice x4, local copies, waits for them, and re-layouts, merged(): tail = jax.tree.map(lambda part: part[1:], pieces)  6.89 us
    add x7, other arithmetic, merge_states(): normal = first[1] * left[..., None] + second[1] * right[..., None]  5.45 us
    unnamed x17, local copies, waits for them, and re-layouts  5.28 us
  transfers between devices with their start and end apart: 2, of which 0 were waited for; matrix products, arithmetic and copies ran while one was open for 3% of the time, Pallas kernels for 0%

commit v1 on v0

v1 whole, which is shorter than its diff:
```python
import jax
import jax.numpy as jnp
from jax import lax
from jax.sharding import PartitionSpec as P

HIGH = lax.Precision.HIGHEST


def local(tokens, key_weight, value_weight, input_weight, forget_weight, forget_bias, query):
    seqs, span, width = tokens.shape
    heads = input_weight.shape[1]
    kdim = key_weight.shape[1] // heads
    vdim = value_weight.shape[1] // heads
    size = lax.axis_size("sp")
    me = lax.axis_index("sp")
    pieces = size // seqs
    sub = span // pieces
    rows = heads * kdim // pieces
    flat = tokens.reshape(seqs * span, width)
    gate_pair = jnp.concatenate([input_weight, forget_weight], axis=1)
    gates = lax.dot_general(gate_pair, flat, (((0,), (1,)), ((), ())), preferred_element_type=jnp.float32)
    igate = gates[:heads]
    logf = jax.nn.log_sigmoid(gates[heads:] + forget_bias[:, None])
    packet = jnp.concatenate([igate, logf]).reshape(2 * heads, seqs, span).transpose(1, 0, 2)
    packet = jnp.repeat(packet, pieces, axis=0)
    packet = lax.all_to_all(packet, "sp", split_axis=0, concat_axis=0, tiled=True)
    values = jnp.dot(flat, value_weight, preferred_element_type=jnp.float32).astype(jnp.bfloat16)
    keys = jnp.dot(flat, key_weight, preferred_element_type=jnp.float32).astype(jnp.bfloat16)
    value_cache = lax.all_to_all(
        values.reshape(size, sub, heads * vdim), "sp", split_axis=0, concat_axis=1, tiled=True
    )
    key_cache = lax.all_to_all(
        keys.reshape(size, sub, heads * kdim), "sp", split_axis=0, concat_axis=1, tiled=True
    )
    igate, logf = packet[:, :heads], packet[:, heads:]
    at = jnp.arange(span)
    behind = (at[:, None] > at[None, :]).astype(jnp.float32)
    after = jnp.einsum("pht,ts->phs", logf, behind, precision=HIGH)
    sums = jnp.sum(logf, axis=2)
    block = jnp.arange(size)
    later = jnp.sum(jnp.where(block[:, None, None] > block[None, :, None], sums[:, None, :], 0.0), axis=0)
    total = jnp.sum(sums, axis=0)
    logw = after + later[:, :, None] + igate
    stabilizer = jnp.maximum(total, jnp.max(logw, axis=(0, 2)))
    mine = lax.dynamic_slice_in_dim(logw, lax.rem(me, pieces) * sub, sub, axis=2)
    weight = jnp.exp(mine - stabilizer[None, :, None]) * kdim ** (-0.5)
    weight = weight.transpose(0, 2, 1).reshape(size * sub, heads, 1)
    scaled = key_cache.reshape(size * sub, heads, kdim).astype(jnp.float32) * weight
    kept = value_cache.reshape(size * sub, heads, vdim).astype(jnp.float32)
    memory = jnp.einsum("lhd,lhe->hde", scaled, kept, precision=HIGH)
    normal = jnp.sum(scaled, axis=0).reshape(pieces, 1, rows)
    fill = jnp.zeros((pieces, 6, vdim), jnp.float32)
    tail = jnp.pad(normal, ((0, 0), (0, 0), (0, vdim - rows)))
    level = jnp.broadcast_to(jnp.pad(stabilizer, (0, vdim - heads)) / pieces, (pieces, 1, vdim))
    share = jnp.concatenate([memory.reshape(pieces, rows, vdim), tail, level, fill], axis=1)
    groups = [[s * pieces + b for b in range(pieces)] for s in range(seqs)]
    share = lax.all_to_all(share, "sp", split_axis=0, concat_axis=0, tiled=True, axis_index_groups=groups)
    share = jnp.sum(share, axis=0)
    every = lax.all_gather(share, "sp").reshape(seqs, pieces, rows + 8, vdim)
    memory = every[:, :, :rows].reshape(seqs, heads, kdim, vdim)
    normalizer = every[:, :, rows, :rows].reshape(seqs, heads, kdim)
    stabilizer = every[:, 0, rows + 1, :heads]
    asked = query.astype(jnp.float32).reshape(seqs, heads, kdim)
    numer = jnp.sum(asked[..., None] * memory, axis=2)
    denom = jnp.maximum(jnp.abs(jnp.sum(asked * normalizer, axis=-1)), 1.0)
    first_read = (numer / denom[..., None]).reshape(seqs, heads * vdim)
    return (key_cache, value_cache, memory, normalizer, stabilizer, first_read)


def solution(mesh):
    return jax.shard_map(
        local,
        mesh=mesh,
        in_specs=(
            P("gr", "sp", None),
            P(None, "tp"),
            P(None, "tp"),
            P(None, "tp"),
            P(None, "tp"),
            P("tp"),
            P("gr", "tp"),
        ),
        out_specs=(
            P(("gr", "sp"), None, "tp"),
            P(("gr", "sp"), None, "tp"),
            P("gr", "tp", None, None),
            P("gr", "tp", None),
            P("gr", "tp"),
            P("gr", "tp"),
        ),
        check_vma=False,
    )
```

time: 213 us -> 116 us (0.54)
  blocking collectives: 111 us -> 32.2 us
  other arithmetic: 40.9 us -> 12.4 us
  waiting for transfers between devices: 0.02 us -> 14 us
  between operations: 14.2 us -> 0.75 us
  starting transfers between devices: 10.2 us -> 19 us
    all_gather x3 -> x1, blocking collectives: 95.8 us -> 32.2 us  [local(): every = lax.all_gather(share, 'sp').reshape(seqs, pieces, rows + 8, vdim)]
    add x22 -> x0, other arithmetic: 25.1 us -> none  [the longest x7 14.8 us: merge_states(): first[0] * left[..., None, None] + second[0] * right[..., None, None]]
    all_to_all x1 -> x0, blocking collectives: 15.3 us -> none  [local(): lax.all_to_all(keys3.reshape(seqs * pieces, sub, heads * kdim), 'sp', spl...]
    all_to_all x1 -> x4, waiting for transfers between devices: 0.01 us -> 14 us  [the longest x1 6.19 us: local(): lax.all_to_all(keys.reshape(size, sub, heads * kdim), 'sp', split_axis=0,...]
    all_to_all x1 -> x4, starting transfers between devices: 10.2 us -> 19 us  [the longest x1 7.31 us: local(): lax.all_to_all(packet, 'sp', split_axis=0, concat_axis=0, tiled=True)]
    slice x10 -> x3, local copies, waits for them, and re-layouts: 9.67 us -> 2.02 us  [the longest x1 0.83 us: local(): memory = every[:, :, :rows].reshape(seqs, heads, kdim, vdim)]
    mul x0 -> x5, local copies, waits for them, and re-layouts: none -> 7.55 us  [the longest x4 6.78 us: local(): key_cache.reshape(size * sub, heads, kdim).astype(jnp.float32) * weight]
    exp x8 -> x0, other arithmetic: 5.39 us -> none  [the longest x7 4.81 us: merge_states(): left = jnp.exp(first[2] - top)]
  transfers between devices with their start and end apart: 2 -> 4, of which waited for: 0 -> 3; matrix products, arithmetic and copies ran while one was open for 3% -> 24% of each run, Pallas kernels for 0% -> 0%
where the time goes in v1:
time: 116 us; the launch traced here: 115 us
  blocking collectives  32.2 us (28%)
  local copies, waits for them, and re-layouts  24.5 us (21%)
  starting transfers between devices  19 us (16%)
  waiting for transfers between devices  14 us (12%)
  other arithmetic  12.4 us (11%)
  matrix products  11.9 us (10%)
    all_gather x1, blocking collectives, local(): every = lax.all_gather(share, 'sp').reshape(seqs, pieces, rows + 8, vdim)  32.2 us
    all_to_all x1, starting transfers between devices, local(): lax.all_to_all(packet, 'sp', split_axis=0, concat_axis=0, tiled=True)  7.31 us
    mul x4, local copies, waits for them, and re-layouts, local(): key_cache.reshape(size * sub, heads, kdim).astype(jnp.float32) * weight  6.78 us
    unnamed x14, local copies, waits for them, and re-layouts  6.52 us
    all_to_all x1, waiting for transfers between devices, local(): lax.all_to_all(keys.reshape(size, sub, heads * kdim), 'sp', split_axis=0,...  6.19 us
    dot_general x1, matrix products, local(): jnp.dot(flat, value_weight, preferred_element_type=jnp.float32)  4.25 us
    all_to_all x1, starting transfers between devices, local(): lax.all_to_all(values.reshape(size, sub, heads * vdim), 'sp', split_axis=...  4.22 us
    all_to_all x1, starting transfers between devices, local(): lax.all_to_all(share, 'sp', split_axis=0, concat_axis=0, tiled=True, axis...  4.05 us
  transfers between devices with their start and end apart: 4, of which 3 were waited for; matrix products, arithmetic and copies ran while one was open for 24% of the time, Pallas kernels for 0%

profile of v1, /device:TPU:0, one launch (start us, length us, event | category | flops | bytes accessed | tf_op | source)
XLA Modules:
  0.0 114.7 jit_solution(10419583039381891415)
XLA Ops:
  0.6 0.0 copy-start
  0.6 0.0 copy-start.3
  0.7 1.9 %copy-done = bf16[4,192,2048]{2,1,0:T(8,128)(2,1)S(1)} copy-done((bf16[4,192,2048]{2,1,0:T(8,128)(2,1)S(1)}, bf16[4,192,2048]{2,1,0:T(8,128)(2,1)}, u32[]{:S(2)}) %copy-start) | copy-done | bytes 3145752
  2.5 1.6 %fusion.7 = f32[8,768]{1,0:T(8,128)S(1)} fusion(bf16[768,2048]{1,0:T(8,128)(2,1)S(1)} %bitcast.37, bf16[2048,4]{0,1:T(4,128)(2,1)} %param.11, bf16[2048,4]{0,1:T(4,128)(2,1)} %param.10), kind=kOutput, calls=%fused_computation.14 | convolution fusion | flops 25231360 | bytes 3203072 | tf_op jit(solution)/shard_map/dot_general | solution.py:21
  4.2 0.0 copy-done.3
  4.2 0.1 fusion.15
  4.3 0.1 reshape.94
  4.4 0.6 broadcast_in_dim.38
  5.1 7.3 %all-to-all-start.2 = ((f32[8,8,192]{2,1,0:T(8,128)}), f32[8,8,192]{2,1,0:T(8,128)S(1)}, u32[]{:S(2)}, u32[]{:S(2)}) async-start(f32[8,8,192]{2,1,0:T(8,128)} %bitcast.6), calls=%async_computation.2 | async-start | bytes 131072 | tf_op jit(solution)/shard_map/all_to_all | solution.py:26
  12.4 3.0 %convolution_convert_fusion.1 = bf16[768,256]{1,0:T(8,128)(2,1)} fusion(bf16[768,2048]{1,0:T(8,128)(2,1)S(1)} %bitcast.35, bf16[2048,256]{1,0:T(8,128)(2,1)} %param.8), kind=kOutput, calls=%fused_computation.1 | convolution fusion | flops 805502976 | bytes 4587520 | tf_op jit(solution)/shard_map/dot_general | solution.py:28
  15.3 4.0 %all-to-all-done.2 = f32[8,8,192]{2,1,0:T(8,128)S(1)} async-done(((f32[8,8,192]{2,1,0:T(8,128)}), f32[8,8,192]{2,1,0:T(8,128)S(1)}, u32[]{:S(2)}, u32[]{:S(2)}) %all-to-all-start.2) | async-done | bytes 49184 | tf_op jit(solution)/shard_map/all_to_all | solution.py:26
  19.3 0.0 copy-start.1
  19.3 0.6 copy-done.1
  19.9 3.5 %all-to-all-start = ((bf16[8,96,256]{2,1,0:T(8,128)(2,1)}), bf16[8,96,256]{2,1,0:T(8,128)(2,1)S(1)}, u32[]{:S(2)}, u32[]{:S(2)}) async-start(bf16[8,96,256]{2,1,0:T(8,128)(2,1)} %bitcast.46), calls=%async_computation | async-start | bytes 786432 | tf_op jit(solution)/shard_map/all_to_all | solution.py:32
  23.4 4.3 %convolution_convert_fusion = bf16[768,512]{1,0:T(8,128)(2,1)} fusion(bf16[768,2048]{1,0:T(8,128)(2,1)S(1)} %bitcast.36, bf16[2048,512]{1,0:T(8,128)(2,1)} %param.9), kind=kOutput, calls=%fused_computation | convolution fusion | flops 1611005952 | bytes 6029312 | tf_op jit(solution)/shard_map/dot_general | solution.py:27
  27.6 6.2 %all-to-all-done = bf16[8,96,256]{2,1,0:T(8,128)(2,1)S(1)} async-done(((bf16[8,96,256]{2,1,0:T(8,128)(2,1)}), bf16[8,96,256]{2,1,0:T(8,128)(2,1)S(1)}, u32[]{:S(2)}, u32[]{:S(2)}) %all-to-all-start) | async-done | bytes 393248 | tf_op jit(solution)/shard_map/all_to_all | solution.py:32
  33.8 4.2 %all-to-all-start.1 = ((bf16[8,96,512]{2,1,0:T(8,128)(2,1)}), bf16[8,96,512]{2,1,0:T(8,128)(2,1)}, u32[]{:S(2)}, u32[]{:S(2)}) async-start(bf16[8,96,512]{2,1,0:T(8,128)(2,1)} %bitcast.44), calls=%async_computation.1 | async-start | bytes 1572864 | tf_op jit(solution)/shard_map/all_to_all | solution.py:29
  38.1 0.1 pad.8.clone
  38.1 0.6 iota_compare_fusion.1
  38.7 2.2 %slice_reduce_fusion.2 = (f32[8,4]{1,0:T(8,128)S(1)}, f32[4]{0:T(128)}, f32[8,4,192]{2,1,0:T(4,128)}, f32[8,4,192]{2,1,0:T(4,128)}) fusion(f32[8,8,192]{2,1,0:T(8,128)} %copy-done.1), kind=kLoop, calls=%fused_computation.34 | loop fusion | flops 12252 | bytes 98448 | tf_op jit(solution)/shard_map/reduce_sum | solution.py:39
  40.9 0.1 copy.38
  40.9 0.8 select_reduce_fusion
  41.7 1.1 fusion.16
  42.8 0.7 max.26
  43.4 0.0 copy-start.4
  43.4 0.5 copy-done.4
  44.0 0.7 multiply_bitcast_fusion
  44.6 0.8 mul.43
  45.4 0.9 mul.44
  46.4 2.6 %mul.46 = f32[8,96,256]{1,0,2:T(8,128)} reshape(f32[768,4,64]{0,2,1:T(8,128)} %mul.44) | data formatting | bytes 1572864 | tf_op jit(solution)/shard_map/mul | solution.py:48
  49.0 2.4 %copy.35 = f32[8,96,256]{2,1,0:T(8,128)} copy(f32[8,96,256]{1,0,2:T(8,128)} %mul.46) | data formatting | bytes 1572864 | tf_op jit(solution)/shard_map/mul | solution.py:48
  51.4 1.2 %pad_multiply_fusion = f32[128]{0:T(128)} fusion(f32[4]{0:T(128)} %copy-done.4), kind=kLoop, calls=%fused_computation.31 | loop fusion | flops 128 | bytes 528 | tf_op jit(solution)/shard_map/div | solution.py:54
  52.6 1.2 %copy.30 = f32[8,96,256]{1,0,2:T(8,128)} copy(bf16[8,96,256]{2,1,0:T(8,128)(2,1)S(1)} %all-to-all-done) | data formatting | bytes 1179648 | tf_op jit(solution)/shard_map/convert_element_type | solution.py:48
  53.8 2.5 %reshape.101 = f32[768,4,64]{0,2,1:T(8,128)} reshape(f32[8,96,256]{1,0,2:T(8,128)} %copy.30) | data formatting | bytes 1572864 | tf_op jit(solution)/shard_map/convert_element_type | solution.py:48
  56.3 1.8 %multiply_reduce_fusion = f32[256]{0:T(256)} fusion(f32[8,96,256]{2,1,0:T(8,128)} %copy.35, bf16[8,96,256]{2,1,0:T(8,128)(2,1)S(1)} %all-to-all-done), kind=kLoop, calls=%fused_computation.6 | loop fusion | flops 589568 | bytes 1180672 | tf_op jit(solution)/shard_map/reduce_sum | solution.py:51
  58.1 0.0 all-to-all-done.1
  58.1 2.4 %reshape.96 = bf16[768,4,128]{2,1,0:T(4,128)(2,1)} reshape(bf16[8,96,512]{2,1,0:T(8,128)(2,1)} %all-to-all-done.1) | data formatting | bytes 1572864 | tf_op jit(solution)/shard_map/reshape | solution.py:49
  60.6 1.9 %fusion.1 = f32[4,64,128]{2,1,0:T(8,128)S(1)} fusion(bf16[768,4,128]{2,1,0:T(4,128)(2,1)} %reshape.96, f32[768,4,64]{0,2,1:T(8,128)} %reshape.101, f32[768,4]{0,1:T(4,128)S(1)} %mul.43), kind=kOutput, calls=%fused_computation.4 | convolution fusion | flops 302186496 | bytes 1716224 | tf_op jit(solution)/shard_map/lhd,lhe->hde/dot_general | solution.py:50
  62.5 0.7 broadcast_in_dim.42
  63.2 1.4 %maximum_maximum_fusion = f32[2,136,128]{2,1,0:T(8,128)} fusion(f32[2,1,128]{2,1,0:T(1,128)S(1)} %broadcast_in_dim.42, f32[2,1,128]{2,1,0:T(1,128)} %bitcast.49, f32[2,128,128]{2,1,0:T(8,128)S(1)} %bitcast.45, f32[136]{0:T(256)S(1)} %pad.8.clone), kind=kLoop, calls=%fused_computation.12 | loop fusion | flops 104448 | bytes 272928 | tf_op jit(solution)/shard_map/concatenate | solution.py:55
  64.6 4.1 %all-to-all-start.3 = ((f32[2,136,128]{2,1,0:T(8,128)}), f32[2,136,128]{2,1,0:T(8,128)}, u32[]{:S(2)}, u32[]{:S(2)}) async-start(f32[2,136,128]{2,1,0:T(8,128)} %maximum_maximum_fusion), calls=%async_computation.3 | async-start | bytes 278528 | tf_op jit(solution)/shard_map/all_to_all | solution.py:57
  68.6 0.8 reshape.102
  69.4 3.8 %all-to-all-done.3 = f32[2,136,128]{2,1,0:T(8,128)} async-done(((f32[2,136,128]{2,1,0:T(8,128)}), f32[2,136,128]{2,1,0:T(8,128)}, u32[]{:S(2)}, u32[]{:S(2)}) %all-to-all-start.3) | async-done | bytes 139296 | tf_op jit(solution)/shard_map/all_to_all | solution.py:57
  73.2 1.6 %reduce_sum.67 = f32[136,128]{1,0:T(8,128)} reduce(f32[2,136,128]{2,1,0:T(8,128)} %all-to-all-done.3, f32[]{:T(128)} %constant.11.clone.1), dimensions={0}, to_apply=%region_5.6 | reduce | flops 17408 | bytes 208900 | tf_op jit(solution)/shard_map/reduce_sum | solution.py:58
  74.8 32.2 %all-gather = f32[1088,128]{1,0:T(8,128)S(1)} all-gather(f32[136,128]{1,0:T(8,128)} %reduce_sum.67), channel_id=2, replica_groups=mesh['gr'=2,'sp'=8,'tp'=2] {'sp'}, dimensions={0}, use_global_device_ids=true | all-gather | bytes 626688 | tf_op jit(solution)/shard_map/all_gather | solution.py:59
  107.0 0.8 slice.32
  107.8 0.6 slice_reduce_fusion
  108.4 0.6 slice.34
  109.0 0.8 reshape_squeeze.3
  109.8 0.0 copy-start.2
  109.8 1.3 %multiply_reduce_fusion.1 = f32[4,4,128]{2,1,0:T(4,128)S(1)} fusion(f32[4,4,64,128]{3,2,1,0:T(8,128)} %bitcast.42, f32[4,4,64]{2,1,0:T(4,128)S(1)} %reshape.102), kind=kLoop, calls=%fused_computation.8 | loop fusion | flops 260096 | bytes 536576 | tf_op jit(solution)/shard_map/reduce_sum | solution.py:64
  111.1 0.1 multiply_reduce_fusion.2
  111.2 0.1 divide_bitcast_fusion
  111.2 0.6 copy.49
  111.8 0.7 copy.52
  112.6 2.1 %copy.53 = bf16[1,768,512]{2,1,0:T(8,128)(2,1)} copy(bf16[1,768,512]{2,1,0:T(8,128)(2,1)} %bitcast.4) | data formatting | bytes 1572864
  114.7 0.0 copy-done.2
  (4 shorter events, 0.0 us)
Async XLA Ops:
  0.6 1.9 %copy-start = (bf16[4,192,2048]{2,1,0:T(8,128)(2,1)S(1)}, bf16[4,192,2048]{2,1,0:T(8,128)(2,1)}, u32[]{:S(2)}) copy-start(bf16[4,192,2048]{2,1,0:T(8,128)(2,1)} %param.7) | copy-start | bytes 9437188
  0.6 3.5 %copy-start.3 = (f32[4]{0:T(128)S(1)}, f32[4]{0:T(128)}, u32[]{:S(2)}) copy-start(f32[4]{0:T(128)} %param.12) | copy-start | bytes 52
  5.1 14.2 %all-to-all-start.2 = ((f32[8,8,192]{2,1,0:T(8,128)}), f32[8,8,192]{2,1,0:T(8,128)S(1)}, u32[]{:S(2)}, u32[]{:S(2)}) async-start(f32[8,8,192]{2,1,0:T(8,128)} %bitcast.6), calls=%async_computation.2 | async-start | bytes 131072 | tf_op jit(solution)/shard_map/all_to_all | solution.py:26
  19.3 0.6 copy-start.1
  19.9 13.9 %all-to-all-start = ((bf16[8,96,256]{2,1,0:T(8,128)(2,1)}), bf16[8,96,256]{2,1,0:T(8,128)(2,1)S(1)}, u32[]{:S(2)}, u32[]{:S(2)}) async-start(bf16[8,96,256]{2,1,0:T(8,128)(2,1)} %bitcast.46), calls=%async_computation | async-start | bytes 786432 | tf_op jit(solution)/shard_map/all_to_all | solution.py:32
  33.8 24.3 %all-to-all-start.1 = ((bf16[8,96,512]{2,1,0:T(8,128)(2,1)}), bf16[8,96,512]{2,1,0:T(8,128)(2,1)}, u32[]{:S(2)}, u32[]{:S(2)}) async-start(bf16[8,96,512]{2,1,0:T(8,128)(2,1)} %bitcast.44), calls=%async_computation.1 | async-start | bytes 1572864 | tf_op jit(solution)/shard_map/all_to_all | solution.py:29
  43.4 0.5 copy-start.4
  64.6 8.7 %all-to-all-start.3 = ((f32[2,136,128]{2,1,0:T(8,128)}), f32[2,136,128]{2,1,0:T(8,128)}, u32[]{:S(2)}, u32[]{:S(2)}) async-start(f32[2,136,128]{2,1,0:T(8,128)} %maximum_maximum_fusion), calls=%async_computation.3 | async-start | bytes 278528 | tf_op jit(solution)/shard_map/all_to_all | solution.py:57
  109.8 4.9 %copy-start.2 = (f32[4,4,64]{2,1,0:T(4,128)}, f32[4,4,64]{2,1,0:T(4,128)S(1)}, u32[]{:S(2)}) copy-start(f32[4,4,64]{2,1,0:T(4,128)S(1)} %reshape_squeeze.3) | copy-start | bytes 12292

commit v2 on v1

--- a/solution.py
+++ b/solution.py
@@ -1,12 +1,16 @@
+import functools
+
 import jax
 import jax.numpy as jnp
 from jax import lax
+from jax.experimental import pallas as pl
+from jax.experimental.pallas import tpu as pltpu
 from jax.sharding import PartitionSpec as P
 
 HIGH = lax.Precision.HIGHEST
 
 
-def local(tokens, key_weight, value_weight, input_weight, forget_weight, forget_bias, query):
+def plain(tokens, key_weight, value_weight, input_weight, forget_weight, forget_bias, query):
     seqs, span, width = tokens.shape
     heads = input_weight.shape[1]
     kdim = key_weight.shape[1] // heads
@@ -67,6 +71,254 @@
     return (key_cache, value_cache, memory, normalizer, stabilizer, first_read)
 
 
+def kernel(
+    dims, tok, kw, vw, gw, bias, query,
+    key_out, val_out, mem_out, norm_out, stab_out, read_out,
+    key_send, val_send, gate_send, gate_got, wide, part, part_got, every,
+    ks, kr, vs, vr, gs, gr, ps, pr, es, fs, er,
+):
+    seqs, span, heads, kdim, vdim, size = dims
+    pieces = size // seqs
+    sub = span // pieces
+    rows = heads * kdim // pieces
+    me = lax.axis_index("sp")
+    seq, piece = me // pieces, me % pieces
+
+    def copy(src, dst, send, recv, to):
+        return pltpu.make_async_remote_copy(
+            src_ref=src, dst_ref=dst, send_sem=send, recv_sem=recv,
+            device_id={"sp": to}, device_id_type=pl.DeviceIdType.MESH,
+        )
+
+    barrier = pltpu.get_barrier_semaphore()
+    for k in range(1, size):
+        pl.semaphore_signal(
+            barrier, inc=1, device_id={"sp": (me + k) % size}, device_id_type=pl.DeviceIdType.MESH
+        )
+    gates = lax.dot_general(
+        tok[...], gw[...], (((1,), (1,)), ((), ())), preferred_element_type=jnp.float32
+    ).T
+    fpre = gates[heads : 2 * heads] + bias[...]
+    logf = jnp.minimum(fpre, 0.0) - jnp.log1p(jnp.exp(-jnp.abs(fpre)))
+    for s in range(seqs):
+        gate_send[s, 0:heads, :] = gates[0:heads, s * span : (s + 1) * span]
+        gate_send[s, heads : 2 * heads, :] = logf[:, s * span : (s + 1) * span]
+    pl.semaphore_wait(barrier, size - 1)
+
+    def gate_copy(k):
+        to = (me + k) % size
+        return copy(gate_send.at[to // pieces], gate_got.at[me], gs.at[to], gr.at[me], to)
+
+    half = seqs // 2
+    up = seq // half
+
+    def key_copy(to):
+        return copy(key_send.at[to], key_out.at[me], ks.at[to], kr.at[me], to)
+
+    def val_copy(to):
+        return copy(val_send.at[to], val_out.at[me], vs.at[to], vr.at[me], to)
+
+    def project(k):
+        off = up * ((k + 1) % seqs) + (1 - up) * (seqs - 1 - k)
+        s = (seq + off) % seqs
+        block = tok[pl.ds(pl.multiple_of(s * span, span), span), :]
+        keys = jnp.dot(block, kw[...], preferred_element_type=jnp.float32).astype(jnp.bfloat16)
+        for b in range(pieces):
+            key_send[s * pieces + b] = keys[b * sub : (b + 1) * sub]
+        values = jnp.dot(block, vw[...], preferred_element_type=jnp.float32).astype(jnp.bfloat16)
+        for b in range(pieces):
+            val_send[s * pieces + b] = values[b * sub : (b + 1) * sub]
+        return s
+
+    def step(k, carry):
+        s = project(k)
+        for b in range(pieces):
+            key_copy(s * pieces + b).start()
+            val_copy(s * pieces + b).start()
+        return carry
+
+    for k in range(1, size):
+        gate_copy(k).start()
+    lax.fori_loop(0, seqs - 1, step, 0)
+    project(seqs - 1)
+    for j in range(1, pieces):
+        to = seq * pieces + (piece + j) % pieces
+        key_copy(to).start()
+        val_copy(to).start()
+    key_out[me] = key_send[me]
+    val_out[me] = val_send[me]
+    gate_got[me] = gate_send[seq]
+
+    for k in range(1, size):
+        src = (me + k) % size
+        copy(gate_send.at[seq], gate_got.at[src], gs.at[src], gr.at[src], src).wait_recv()
+    got = gate_got[...]
+    flat = got.reshape(size * 2 * heads, span)
+    row = lax.broadcasted_iota(jnp.int32, (span, span), 0)
+    col = lax.broadcasted_iota(jnp.int32, (span, span), 1)
+    behind = jnp.where(row > col, 1.0, 0.0).astype(jnp.float32)
+    after = jnp.dot(flat, behind, precision=HIGH, preferred_element_type=jnp.float32)
+    after = after.reshape(size, 2 * heads, span)
+    later = jnp.zeros((heads, 1), jnp.float32)
+    logw = [None] * size
+    for p in range(size - 1, -1, -1):
+        logw[p] = after[p, heads:] + later + got[p, :heads]
+        later = later + jnp.sum(got[p, heads:], axis=1, keepdims=True)
+    top = functools.reduce(jnp.maximum, logw)
+    stab = jnp.maximum(later, jnp.max(top, axis=1, keepdims=True))
+    lane = lax.broadcasted_iota(jnp.int32, (2 * heads, heads * kdim), 1)
+    head = lax.broadcasted_iota(jnp.int32, (2 * heads, heads * kdim), 0)
+    spread = jnp.where((lane >= head * kdim) & (lane < (head + 1) * kdim), 1.0, 0.0).astype(jnp.float32)
+    for p in range(size):
+        weight = jnp.exp(logw[p] - stab) * kdim ** (-0.5)
+        mine = weight[:, 0:sub]
+        for b in range(1, pieces):
+            mine = jnp.where(piece == b, weight[:, b * sub : (b + 1) * sub], mine)
+        mine = jnp.concatenate([mine, jnp.zeros_like(mine)], axis=0).T
+        wide[p] = jnp.dot(mine, spread, precision=HIGH, preferred_element_type=jnp.float32)
+
+    for k in range(1, size):
+        src = (me + k) % size
+        copy(key_send.at[src], key_out.at[src], ks.at[src], kr.at[src], src).wait_recv()
+        copy(val_send.at[src], val_out.at[src], vs.at[src], vr.at[src], src).wait_recv()
+    scaled = key_out[...].astype(jnp.float32) * wide[...]
+    scaled = scaled.reshape(size * sub, heads * kdim)
+    normal = jnp.sum(scaled, axis=0, keepdims=True)
+    turned = scaled.T
+    high = turned.astype(jnp.bfloat16)
+    low = (turned - high.astype(jnp.float32)).astype(jnp.bfloat16)
+    kept = val_out[...].reshape(size * sub, heads * vdim)
+    cross = jnp.dot(high, kept, preferred_element_type=jnp.float32)
+    cross = cross + jnp.dot(low, kept, preferred_element_type=jnp.float32)
+    per = heads // pieces
+    for h in range(heads):
+        at = (h % per) * kdim
+        part[h // per, at : at + kdim, :] = cross[h * kdim : (h + 1) * kdim, h * vdim : (h + 1) * vdim]
+    for b in range(pieces):
+        part[b, rows : rows + 8, 0:rows] = jnp.broadcast_to(normal[:, b * rows : (b + 1) * rows], (8, rows))
+        part[b, rows + 8 : rows + 16, :] = jnp.zeros((8, vdim), jnp.float32)
+
+    for j in range(1, pieces):
+        other = (piece + j) % pieces
+        to = seq * pieces + other
+        copy(part.at[other], part_got.at[piece], ps.at[other], pr.at[piece], to).start()
+    share = part[piece]
+    for j in range(1, pieces):
+        other = (piece + j) % pieces
+        to = seq * pieces + other
+        copy(part.at[other], part_got.at[other], ps.at[other], pr.at[other], to).wait_recv()
+        share = share + part_got[other]
+    every[me] = share
+    every[me, rows + 8 : rows + 8 + heads, :] = jnp.broadcast_to(stab, (heads, vdim))
+
+    def across(k):
+        to = ((seq + k) % seqs) * pieces + piece
+        return copy(every.at[me], every.at[me], es.at[k], er.at[me], to)
+
+    def along(k, j):
+        src = ((seq + k) % seqs) * pieces + piece
+        to = seq * pieces + (piece + j) % pieces
+        return copy(every.at[src], every.at[src], fs.at[k, j], er.at[src], to)
+
+    def landed(src):
+        copy(every.at[src], every.at[src], es.at[0], er.at[src], src).wait_recv()
+
+    for k in range(1, seqs):
+        across(k).start()
+    for j in range(1, pieces):
+        along(0, j).start()
+    for k in range(1, seqs):
+        landed(((seq + k) % seqs) * pieces + piece)
+        for j in range(1, pieces):
+            along(k, j).start()
+    for k in range(seqs):
+        for j in range(1, pieces):
+            landed(((seq + k) % seqs) * pieces + (piece + j) % pieces)
+
+    asked = query[...].astype(jnp.float32)
+    select = spread[0:heads]
+    for s in range(seqs):
+        for b in range(pieces):
+            mem_out[s, b * rows : (b + 1) * rows, :] = every[s * pieces + b, 0:rows, :]
+            norm_out[s : s + 1, b * rows : (b + 1) * rows] = every[s * pieces + b, rows : rows + 1, 0:rows]
+        stab_out[s] = every[s * pieces, rows + 8 : rows + 8 + heads, :]
+        one = asked[s : s + 1] * select
+        numer = jnp.dot(one, mem_out[s], precision=HIGH, preferred_element_type=jnp.float32)
+        inner = jnp.sum(one * norm_out[s : s + 1, :], axis=1, keepdims=True)
+        read = numer / jnp.maximum(jnp.abs(inner), 1.0)
+        for h in range(heads):
+            read_out[s : s + 1, h * vdim : (h + 1) * vdim] = read[h : h + 1]
+
+    for k in range(1, size):
+        gate_copy(k).wait_send()
+        key_copy((me + k) % size).wait_send()
+        val_copy((me + k) % size).wait_send()
+    for j in range(1, pieces):
+        other = (piece + j) % pieces
+        copy(part.at[other], part_got.at[piece], ps.at[other], pr.at[piece], seq * pieces + other).wait_send()
+    for k in range(1, seqs):
+        across(k).wait_send()
+    for k in range(seqs):
+        for j in range(1, pieces):
+            along(k, j).wait_send()
+
+
+def local(tokens, key_weight, value_weight, input_weight, forget_weight, forget_bias, query):
+    seqs, span, width = tokens.shape
+    heads = input_weight.shape[1]
+    kdim = key_weight.shape[1] // heads
+    vdim = value_weight.shape[1] // heads
+    size = lax.axis_size("sp")
+    pieces = size // seqs
+    sub = span // pieces
+    rows = heads * kdim // pieces
+    fits = heads == 4 and pieces > 1 and heads % pieces == 0 and sub % 16 == 0 and seqs % 2 == 0
+    if not fits or rows % 128 or rows > vdim or vdim % 128:
+        return plain(tokens, key_weight, value_weight, input_weight, forget_weight, forget_bias, query)
+    gates = jnp.concatenate([input_weight.T, forget_weight.T], axis=0)
+    gates = jnp.pad(gates, ((0, 128 - 2 * heads), (0, 0)))
+    f32, bf16 = jnp.float32, jnp.bfloat16
+    vmem = pl.BlockSpec(memory_space=pltpu.VMEM)
+    dma = pltpu.SemaphoreType.DMA
+    outs = pl.pallas_call(
+        functools.partial(kernel, (seqs, span, heads, kdim, vdim, size)),
+        out_shape=(
+            jax.ShapeDtypeStruct((size, sub, heads * kdim), bf16),
+            jax.ShapeDtypeStruct((size, sub, heads * vdim), bf16),
+            jax.ShapeDtypeStruct((seqs, heads * kdim, vdim), f32),
+            jax.ShapeDtypeStruct((seqs, heads * kdim), f32),
+            jax.ShapeDtypeStruct((seqs, heads, vdim), f32),
+            jax.ShapeDtypeStruct((seqs, heads * vdim), f32),
+        ),
+        in_specs=[vmem] * 6,
+        out_specs=(vmem,) * 6,
+        scratch_shapes=[
+            pltpu.VMEM((size, sub, heads * kdim), bf16),
+            pltpu.VMEM((size, sub, heads * vdim), bf16),
+            pltpu.VMEM((seqs, 2 * heads, span), f32),
+            pltpu.VMEM((size, 2 * heads, span), f32),
+            pltpu.VMEM((size, sub, heads * kdim), f32),
+            pltpu.VMEM((pieces, rows + 16, vdim), f32),
+            pltpu.VMEM((pieces, rows + 16, vdim), f32),
+            pltpu.VMEM((size, rows + 16, vdim), f32),
+            dma((size,)), dma((size,)), dma((size,)), dma((size,)), dma((size,)), dma((size,)),
+            dma((pieces,)), dma((pieces,)), dma((seqs,)), dma((seqs, pieces)), dma((size,)),
+        ],
+        compiler_params=pltpu.CompilerParams(
+            collective_id=0, has_side_effects=True, vmem_limit_bytes=48 * 1024 * 1024
+        ),
+    )(tokens.reshape(seqs * span, width), key_weight, value_weight, gates, forget_bias[:, None], query)
+    keys, values, memory, normalizer, level, first_read = outs
+    return (
+        keys.reshape(1, size * sub, heads * kdim),
+        values.reshape(1, size * sub, heads * vdim),
+        memory.reshape(seqs, heads, kdim, vdim),
+        normalizer.reshape(seqs, heads, kdim),
+        level[:, :, 0],
+        first_read,
+    )
+
+
 def solution(mesh):
     return jax.shard_map(
         local,

time: 116 us -> 61.8 us (0.53)
  Pallas kernels: 0 us -> 50.9 us
  blocking collectives: 32.2 us -> 0 us
  starting transfers between devices: 19 us -> 0 us
  local copies, waits for them, and re-layouts: 24.5 us -> 8.59 us
  waiting for transfers between devices: 14 us -> 0 us
  matrix products: 11.9 us -> 0 us
  other arithmetic: 12.4 us -> 0.78 us
    pallas_call x0 -> x1, Pallas kernels: none -> 50.9 us  [local(): pl.pallas_call(functools.partial(kernel, (seqs, span, heads, kdim, vdim,...]
    all_gather x1 -> x0, blocking collectives: 32.2 us -> none  [local(): every = lax.all_gather(share, 'sp').reshape(seqs, pieces, rows + 8, vdim)]
    all_to_all x4 -> x0, starting transfers between devices: 19 us -> none  [the longest x1 7.31 us: local(): lax.all_to_all(packet, 'sp', split_axis=0, concat_axis=0, tiled=True)]
    all_to_all x4 -> x0, waiting for transfers between devices: 14 us -> none  [the longest x1 6.19 us: local(): lax.all_to_all(keys.reshape(size, sub, heads * kdim), 'sp', split_axis=0,...]
    dot_general x5 -> x0, matrix products: 11.9 us -> none  [the longest x1 4.25 us: local(): jnp.dot(flat, value_weight, preferred_element_type=jnp.float32)]
    reduce_sum x6 -> x0, other arithmetic: 7.66 us -> none  [the longest x1 2.16 us: local(): sums = jnp.sum(logf, axis=2)]
    mul x5 -> x0, local copies, waits for them, and re-layouts: 7.55 us -> none  [the longest x4 6.78 us: local(): key_cache.reshape(size * sub, heads, kdim).astype(jnp.float32) * weight]
    convert_element_type x2 -> x0, local copies, waits for them, and re-layouts: 3.69 us -> none  [local(): key_cache.reshape(size * sub, heads, kdim).astype(jnp.float32) * weight]
  transfers between devices with their start and end apart: 4 -> 0, of which waited for: 3 -> 0; matrix products, arithmetic and copies ran while one was open for 24% -> 0% of each run, Pallas kernels for 0% -> 0%
where the time goes in v2:
time: 61.8 us; the launch traced here: 60.9 us
  Pallas kernels  50.9 us (82%)
  local copies, waits for them, and re-layouts  8.59 us (14%)
  other arithmetic  0.78 us (1%)
  between operations  0.66 us (1%)
    pallas_call x1, Pallas kernels, local(): pl.pallas_call(functools.partial(kernel, (seqs, span, heads, kdim, vdim,...  50.9 us
    unnamed x10, local copies, waits for them, and re-layouts  6.51 us

profile of v2, /device:TPU:0, one launch (start us, length us, event | category | flops | bytes accessed | tf_op | source)
XLA Modules:
  0.0 60.9 jit_solution(6778963028638400358)
XLA Ops:
  0.6 0.7 %copy.14.bias = f32[4,1]{1,0:T(4,128)S(1)} copy(f32[4,1]{0,1:T(1,128)} %bitcast.13) | data formatting | bytes 32 | tf_op jit(solution)/shard_map/broadcast_in_dim | solution.py:310
  1.4 0.8 %fusion.2.gw = bf16[128,2048]{1,0:T(8,128)(2,1)S(1)} fusion(bf16[4,2048]{1,0:T(4,128)(2,1)} %bitcast.11, bf16[4,2048]{1,0:T(4,128)(2,1)} %bitcast.12), kind=kLoop, calls=%fused_computation.3 | loop fusion | flops 1835008 | bytes 557056 | tf_op jit(solution)/shard_map/concatenate | solution.py:278
  2.2 0.0 copy-start
  2.2 1.6 %copy-done = bf16[2048,512]{1,0:T(8,128)(2,1)S(1)} copy-done((bf16[2048,512]{1,0:T(8,128)(2,1)S(1)}, bf16[2048,512]{1,0:T(8,128)(2,1)}, u32[]{:S(2)}) %copy-start) | copy-done | bytes 2097176
  3.8 0.0 copy-start.1
  3.8 1.2 %copy-done.1 = bf16[2048,256]{1,0:T(8,128)(2,1)S(1)} copy-done((bf16[2048,256]{1,0:T(8,128)(2,1)S(1)}, bf16[2048,256]{1,0:T(8,128)(2,1)}, u32[]{:S(2)}) %copy-start.1) | copy-done | bytes 1048600
  5.0 0.0 copy-start.2
  5.0 0.7 %copy-done.2 = bf16[4,256]{1,0:T(4,128)(2,1)S(1)} copy-done((bf16[4,256]{1,0:T(4,128)(2,1)S(1)}, bf16[4,256]{1,0:T(4,128)(2,1)}, u32[]{:S(2)}) %copy-start.2) | copy-done | bytes 2072
  5.7 50.9 %shard_map.118 = (bf16[8,96,256]{2,1,0:T(8,128)(2,1)S(1)}, bf16[8,96,512]{2,1,0:T(8,128)(2,1)S(1)}, f32[4,256,128]{2,1,0:T(8,128)S(1)}, f32[4,256]{1,0:T(4,128)S...) custom-call(bf16[768,2048]{1,0:T(8,128)(2,1)} %bitcast.10, bf16[2048,256]{1,0:T(8,128)(2,1)S(1)} %copy-done.1, ...), custom_call_target="tpu_custom_call" | custom-call | tf_op jit(solution)/shard_map/pallas_call | solution.py:283
  56.6 0.7 %slice_reduce_fusion = f32[4,4]{1,0:T(4,128)} fusion(f32[4,4,128]{2,1,0:T(4,128)S(1)} %get-tuple-element.16), kind=kLoop, calls=%fused_computation.4 | loop fusion | bytes 128 | tf_op jit(solution)/shard_map/slice | solution.py:317
  57.2 0.7 %reshape.31 = f32[4,4,64]{2,1,0:T(4,128)} reshape(f32[4,256]{1,0:T(4,128)S(1)} %get-tuple-element.15) | data formatting | bytes 8192 | tf_op jit(solution)/shard_map/reshape | solution.py:316
  57.9 0.7 %copy.19 = bf16[1,768,256]{2,1,0:T(8,128)(2,1)} copy(bf16[1,768,256]{2,1,0:T(8,128)(2,1)S(1)} %bitcast.9) | data formatting | bytes 786432
  58.6 0.9 %copy.20 = bf16[1,768,512]{2,1,0:T(8,128)(2,1)} copy(bf16[1,768,512]{2,1,0:T(8,128)(2,1)S(1)} %bitcast.7) | data formatting | bytes 1572864
  59.5 0.8 %copy.21 = f32[4,4,64,128]{3,2,1,0:T(8,128)} copy(f32[4,4,64,128]{3,2,1,0:T(8,128)S(1)} %bitcast.8) | data formatting | bytes 1048576
  60.3 0.6 copy.22
Async XLA Ops:
  2.2 1.6 %copy-start = (bf16[2048,512]{1,0:T(8,128)(2,1)S(1)}, bf16[2048,512]{1,0:T(8,128)(2,1)}, u32[]{:S(2)}) copy-start(bf16[2048,512]{1,0:T(8,128)(2,1)} %vw.1) | copy-start | bytes 6291460
  3.8 1.2 %copy-start.1 = (bf16[2048,256]{1,0:T(8,128)(2,1)S(1)}, bf16[2048,256]{1,0:T(8,128)(2,1)}, u32[]{:S(2)}) copy-start(bf16[2048,256]{1,0:T(8,128)(2,1)} %kw.1) | copy-start | bytes 3145732
  5.0 0.7 %copy-start.2 = (bf16[4,256]{1,0:T(4,128)(2,1)S(1)}, bf16[4,256]{1,0:T(4,128)(2,1)}, u32[]{:S(2)}) copy-start(bf16[4,256]{1,0:T(4,128)(2,1)} %query.1) | copy-start | bytes 6148

commit v3 on v2

--- a/solution.py
+++ b/solution.py
@@ -73,8 +73,9 @@
 
 def kernel(
     dims, tok, kw, vw, gw, bias, query,
-    key_out, val_out, mem_out, norm_out, stab_out, read_out,
-    key_send, val_send, gate_send, gate_got, wide, part, part_got, every,
+    key_hbm, val_hbm, mem_out, norm_out, stab_out, read_out,
+    key_out, val_out, tokens, key_w, val_w, key_send, val_send, gate_send, gate_got, wide, cross, part, part_got, every,
+    hs, ts, ws,
     ks, kr, vs, vr, gs, gr, ps, pr, es, fs, er,
 ):
     seqs, span, heads, kdim, vdim, size = dims
@@ -90,27 +91,33 @@
             device_id={"sp": to}, device_id_type=pl.DeviceIdType.MESH,
         )
 
+    half = seqs // 2
+    up = seq // half
+
+    def turn(k):
+        off = up * ((k + 1) % seqs) + (1 - up) * (seqs - 1 - k)
+        return (seq + off) % seqs
+
+    def load(k):
+        at = pl.ds(pl.multiple_of(turn(k) * span, span), span)
+        return pltpu.make_async_copy(tok.at[at], tokens.at[at], ts.at[k])
+
+    key_load = pltpu.make_async_copy(kw, key_w, ws.at[0])
+    val_load = pltpu.make_async_copy(vw, val_w, ws.at[1])
+    load(0).start()
+    key_load.start()
+    val_load.start()
+    for k in range(1, seqs):
+        load(k).start()
     barrier = pltpu.get_barrier_semaphore()
     for k in range(1, size):
         pl.semaphore_signal(
             barrier, inc=1, device_id={"sp": (me + k) % size}, device_id_type=pl.DeviceIdType.MESH
         )
-    gates = lax.dot_general(
-        tok[...], gw[...], (((1,), (1,)), ((), ())), preferred_element_type=jnp.float32
-    ).T
-    fpre = gates[heads : 2 * heads] + bias[...]
-    logf = jnp.minimum(fpre, 0.0) - jnp.log1p(jnp.exp(-jnp.abs(fpre)))
-    for s in range(seqs):
-        gate_send[s, 0:heads, :] = gates[0:heads, s * span : (s + 1) * span]
-        gate_send[s, heads : 2 * heads, :] = logf[:, s * span : (s + 1) * span]
     pl.semaphore_wait(barrier, size - 1)
 
-    def gate_copy(k):
-        to = (me + k) % size
+    def gate_copy(to):
         return copy(gate_send.at[to // pieces], gate_got.at[me], gs.at[to], gr.at[me], to)
-
-    half = seqs // 2
-    up = seq // half
 
     def key_copy(to):
         return copy(key_send.at[to], key_out.at[me], ks.at[to], kr.at[me], to)
@@ -119,30 +126,39 @@
         return copy(val_send.at[to], val_out.at[me], vs.at[to], vr.at[me], to)
 
     def project(k):
-        off = up * ((k + 1) % seqs) + (1 - up) * (seqs - 1 - k)
-        s = (seq + off) % seqs
-        block = tok[pl.ds(pl.multiple_of(s * span, span), span), :]
-        keys = jnp.dot(block, kw[...], preferred_element_type=jnp.float32).astype(jnp.bfloat16)
+        s = turn(k)
+        load(k).wait()
+        block = tokens[pl.ds(pl.multiple_of(s * span, span), span), :]
+        keys = jnp.dot(block, key_w[...], preferred_element_type=jnp.float32).astype(jnp.bfloat16)
         for b in range(pieces):
             key_send[s * pieces + b] = keys[b * sub : (b + 1) * sub]
-        values = jnp.dot(block, vw[...], preferred_element_type=jnp.float32).astype(jnp.bfloat16)
+        gates = lax.dot_general(
+            block, gw[...], (((1,), (1,)), ((), ())), preferred_element_type=jnp.float32
+        ).T
+        fpre = gates[heads : 2 * heads] + bias[...]
+        gate_send[s, 0:heads, :] = gates[0:heads]
+        gate_send[s, heads : 2 * heads, :] = jnp.minimum(fpre, 0.0) - jnp.log1p(jnp.exp(-jnp.abs(fpre)))
+        values = jnp.dot(block, val_w[...], preferred_element_type=jnp.float32).astype(jnp.bfloat16)
         for b in range(pieces):
             val_send[s * pieces + b] = values[b * sub : (b + 1) * sub]
         return s
 
     def step(k, carry):
         s = project(k)
+        for b in range(pieces):
+            gate_copy(s * pieces + b).start()
         for b in range(pieces):
             key_copy(s * pieces + b).start()
             val_copy(s * pieces + b).start()
         return carry
 
-    for k in range(1, size):
-        gate_copy(k).start()
+    key_load.wait()
+    val_load.wait()
     lax.fori_loop(0, seqs - 1, step, 0)
     project(seqs - 1)
     for j in range(1, pieces):
         to = seq * pieces + (piece + j) % pieces
+        gate_copy(to).start()
         key_copy(to).start()
         val_copy(to).start()
     key_out[me] = key_send[me]
@@ -177,19 +193,32 @@
         mine = jnp.concatenate([mine, jnp.zeros_like(mine)], axis=0).T
         wide[p] = jnp.dot(mine, spread, precision=HIGH, preferred_element_type=jnp.float32)
 
-    for k in range(1, size):
-        src = (me + k) % size
-        copy(key_send.at[src], key_out.at[src], ks.at[src], kr.at[src], src).wait_recv()
-        copy(val_send.at[src], val_out.at[src], vs.at[src], vr.at[src], src).wait_recv()
-    scaled = key_out[...].astype(jnp.float32) * wide[...]
-    scaled = scaled.reshape(size * sub, heads * kdim)
-    normal = jnp.sum(scaled, axis=0, keepdims=True)
-    turned = scaled.T
-    high = turned.astype(jnp.bfloat16)
-    low = (turned - high.astype(jnp.float32)).astype(jnp.bfloat16)
-    kept = val_out[...].reshape(size * sub, heads * vdim)
-    cross = jnp.dot(high, kept, preferred_element_type=jnp.float32)
-    cross = cross + jnp.dot(low, kept, preferred_element_type=jnp.float32)
+    normal = jnp.zeros((1, heads * kdim), jnp.float32)
+    for k in range(seqs - 1, -1, -1):
+        first = turn(k) * pieces
+        for j in range(pieces):
+            if k == seqs - 1 and j == 0:
+                continue
+            src = first + (piece + j) % pieces
+            copy(key_send.at[src], key_out.at[src], ks.at[src], kr.at[src], src).wait_recv()
+            copy(val_send.at[src], val_out.at[src], vs.at[src], vr.at[src], src).wait_recv()
+        group = pl.ds(first, pieces)
+        scaled = key_out[group].astype(jnp.float32) * wide[group]
+        scaled = scaled.reshape(span, heads * kdim)
+        normal = normal + jnp.sum(scaled, axis=0, keepdims=True)
+        turned = scaled.T
+        high = turned.astype(jnp.bfloat16)
+        low = (turned - high.astype(jnp.float32)).astype(jnp.bfloat16)
+        kept = val_out[group].reshape(span, heads * vdim)
+        term = jnp.dot(high, kept, preferred_element_type=jnp.float32)
+        term = term + jnp.dot(low, kept, preferred_element_type=jnp.float32)
+        cross[...] = term if k == seqs - 1 else cross[...] + term
+    keep = (
+        pltpu.make_async_copy(key_out, key_hbm, hs.at[0]),
+        pltpu.make_async_copy(val_out, val_hbm, hs.at[1]),
+    )
+    for one in keep:
+        one.start()
     per = heads // pieces
     for h in range(heads):
         at = (h % per) * kdim
@@ -237,20 +266,28 @@
 
     asked = query[...].astype(jnp.float32)
     select = spread[0:heads]
+    wide_row = lax.broadcasted_iota(jnp.int32, (heads, vdim), 0)
+    diagonal = lax.broadcasted_iota(jnp.int32, (heads, vdim), 1) == wide_row
     for s in range(seqs):
         for b in range(pieces):
             mem_out[s, b * rows : (b + 1) * rows, :] = every[s * pieces + b, 0:rows, :]
-            norm_out[s : s + 1, b * rows : (b + 1) * rows] = every[s * pieces + b, rows : rows + 1, 0:rows]
-        stab_out[s] = every[s * pieces, rows + 8 : rows + 8 + heads, :]
-        one = asked[s : s + 1] * select
-        numer = jnp.dot(one, mem_out[s], precision=HIGH, preferred_element_type=jnp.float32)
-        inner = jnp.sum(one * norm_out[s : s + 1, :], axis=1, keepdims=True)
+        level = every[s * pieces, rows + 8 : rows + 8 + heads, :]
+        level = jnp.sum(jnp.where(diagonal, level, 0.0), axis=0, keepdims=True)
+        stab_out[s : s + 1, :] = level[:, 0:heads]
+        normal = jnp.concatenate([every[s * pieces + b, rows : rows + 1, 0:rows] for b in range(pieces)], axis=1)
+        for h in range(heads):
+            norm_out[s, h : h + 1, :] = normal[:, h * kdim : (h + 1) * kdim]
+        picked = asked[s : s + 1] * select
+        numer = jnp.dot(picked, mem_out[s], precision=HIGH, preferred_element_type=jnp.float32)
+        inner = jnp.sum(picked * normal, axis=1, keepdims=True)
         read = numer / jnp.maximum(jnp.abs(inner), 1.0)
         for h in range(heads):
             read_out[s : s + 1, h * vdim : (h + 1) * vdim] = read[h : h + 1]
 
+    for one in keep:
+        one.wait()
     for k in range(1, size):
-        gate_copy(k).wait_send()
+        gate_copy((me + k) % size).wait_send()
         key_copy((me + k) % size).wait_send()
         val_copy((me + k) % size).wait_send()
     for j in range(1, pieces):
@@ -261,6 +298,22 @@
     for k in range(seqs):
         for j in range(1, pieces):
             along(k, j).wait_send()
+
+
+def write_out(k_in, v_in, m_in, n_in, s_in, r_in, k_out, v_out, m_out, n_out, s_out, r_out, kb, vb, mb, reads, writes):
+    chain = ((v_in, vb, v_out), (m_in, mb, m_out), (k_in, kb, k_out))
+    ins = [pltpu.make_async_copy(a, b, reads.at[i]) for i, (a, b, c) in enumerate(chain)]
+    outs = [pltpu.make_async_copy(b, c, writes.at[i]) for i, (a, b, c) in enumerate(chain)]
+    for one in ins:
+        one.start()
+    n_out[...] = n_in[...]
+    s_out[...] = s_in[...]
+    r_out[...] = r_in[...]
+    for first, then in zip(ins, outs):
+        first.wait()
+        then.start()
+    for one in outs:
+        one.wait()
 
 
 def local(tokens, key_weight, value_weight, input_weight, forget_weight, forget_bias, query):
@@ -276,9 +329,10 @@
     if not fits or rows % 128 or rows > vdim or vdim % 128:
         return plain(tokens, key_weight, value_weight, input_weight, forget_weight, forget_bias, query)
     gates = jnp.concatenate([input_weight.T, forget_weight.T], axis=0)
-    gates = jnp.pad(gates, ((0, 128 - 2 * heads), (0, 0)))
+    gates = jnp.pad(gates, ((0, 8 * heads - 2 * heads), (0, 0)))
     f32, bf16 = jnp.float32, jnp.bfloat16
     vmem = pl.BlockSpec(memory_space=pltpu.VMEM)
+    hbm = pl.BlockSpec(memory_space=pltpu.HBM)
     dma = pltpu.SemaphoreType.DMA
     outs = pl.pallas_call(
         functools.partial(kernel, (seqs, span, heads, kdim, vdim, size)),
@@ -286,35 +340,51 @@
             jax.ShapeDtypeStruct((size, sub, heads * kdim), bf16),
             jax.ShapeDtypeStruct((size, sub, heads * vdim), bf16),
             jax.ShapeDtypeStruct((seqs, heads * kdim, vdim), f32),
-            jax.ShapeDtypeStruct((seqs, heads * kdim), f32),
-            jax.ShapeDtypeStruct((seqs, heads, vdim), f32),
+            jax.ShapeDtypeStruct((seqs, heads, kdim), f32),
+            jax.ShapeDtypeStruct((seqs, heads), f32),
             jax.ShapeDtypeStruct((seqs, heads * vdim), f32),
         ),
-        in_specs=[vmem] * 6,
-        out_specs=(vmem,) * 6,
+        in_specs=[hbm] * 3 + [vmem] * 3,
+        out_specs=(hbm,) * 2 + (vmem,) * 4,
         scratch_shapes=[
+            pltpu.VMEM((size, sub, heads * kdim), bf16),
+            pltpu.VMEM((size, sub, heads * vdim), bf16),
+            pltpu.VMEM((seqs * span, width), bf16),
+            pltpu.VMEM(key_weight.shape, bf16),
+            pltpu.VMEM(value_weight.shape, bf16),
             pltpu.VMEM((size, sub, heads * kdim), bf16),
             pltpu.VMEM((size, sub, heads * vdim), bf16),
             pltpu.VMEM((seqs, 2 * heads, span), f32),
             pltpu.VMEM((size, 2 * heads, span), f32),
             pltpu.VMEM((size, sub, heads * kdim), f32),
+            pltpu.VMEM((heads * kdim, heads * vdim), f32),
             pltpu.VMEM((pieces, rows + 16, vdim), f32),
             pltpu.VMEM((pieces, rows + 16, vdim), f32),
             pltpu.VMEM((size, rows + 16, vdim), f32),
+            dma((2,)), dma((seqs,)), dma((2,)),
             dma((size,)), dma((size,)), dma((size,)), dma((size,)), dma((size,)), dma((size,)),
             dma((pieces,)), dma((pieces,)), dma((seqs,)), dma((seqs, pieces)), dma((size,)),
         ],
         compiler_params=pltpu.CompilerParams(
-            collective_id=0, has_side_effects=True, vmem_limit_bytes=48 * 1024 * 1024
+            collective_id=0, has_side_effects=True, vmem_limit_bytes=63 * 1024 * 1024
         ),
     )(tokens.reshape(seqs * span, width), key_weight, value_weight, gates, forget_bias[:, None], query)
-    keys, values, memory, normalizer, level, first_read = outs
+    outs = pl.pallas_call(
+        write_out,
+        out_shape=tuple(jax.ShapeDtypeStruct(x.shape, x.dtype) for x in outs),
+        in_specs=[hbm] * 3 + [vmem] * 3,
+        out_specs=(hbm,) * 3 + (vmem,) * 3,
+        scratch_shapes=[pltpu.VMEM(x.shape, x.dtype) for x in (outs[0], outs[1], outs[2])]
+        + [dma((3,)), dma((3,))],
+        compiler_params=pltpu.CompilerParams(vmem_limit_bytes=63 * 1024 * 1024),
+    )(*outs)
+    keys, values, memory, normalizer, stabilizer, first_read = outs
     return (
         keys.reshape(1, size * sub, heads * kdim),
         values.reshape(1, size * sub, heads * vdim),
         memory.reshape(seqs, heads, kdim, vdim),
-        normalizer.reshape(seqs, heads, kdim),
-        level[:, :, 0],
+        normalizer,
+        stabilizer,
         first_read,
     )
 

time: 61.8 us -> 62.3 us (level)
  Pallas kernels: 50.9 us -> 58.5 us
  local copies, waits for them, and re-layouts: 8.59 us -> 1.31 us
  other arithmetic: 0.78 us -> 1.41 us
    unnamed x10 -> x0, local copies, waits for them, and re-layouts: 6.51 us -> none
    pallas_call x1, Pallas kernels: 50.9 us -> 54.8 us  [local(): pl.pallas_call(functools.partial(kernel, (seqs, span, heads, kdim, vdim,...]
    pallas_call x0 -> x1, Pallas kernels: none -> 3.69 us  [local(): pl.pallas_call(write_out, out_shape=tuple((jax.ShapeDtypeStruct(x.shape,...]
    reshape x1 -> x0, local copies, waits for them, and re-layouts: 0.68 us -> none  [local(): normalizer.reshape(seqs, heads, kdim)]
    slice x1 -> x0, local copies, waits for them, and re-layouts: 0.67 us -> none  [local(): level[:, :, 0]]
    concatenate x1, other arithmetic: 0.78 us -> 1.41 us  [local(): gates = jnp.concatenate([input_weight.T, forget_weight.T], axis=0)]
where the time goes in v3:
time: 62.3 us; the launch traced here: 61.9 us
  Pallas kernels  58.5 us (94%)
  other arithmetic  1.41 us (2%)
  local copies, waits for them, and re-layouts  1.31 us (2%)
  between operations  0.64 us (1%)
    pallas_call x1, Pallas kernels, local(): pl.pallas_call(functools.partial(kernel, (seqs, span, heads, kdim, vdim,...  54.8 us
    pallas_call x1, Pallas kernels, local(): pl.pallas_call(write_out, out_shape=tuple((jax.ShapeDtypeStruct(x.shape,...  3.69 us
    concatenate x1, other arithmetic, local(): gates = jnp.concatenate([input_weight.T, forget_weight.T], axis=0)  1.41 us
    broadcast_in_dim x1, local copies, waits for them, and re-layouts, local(): forget_bias[:, None]  1.31 us

profile of v3, /device:TPU:0, one launch (start us, length us, event | category | flops | bytes accessed | tf_op | source)
XLA Modules:
  0.0 61.9 jit_solution(6753359439364593691)
XLA Ops:
  0.6 1.3 %copy.13.bias = f32[4,1]{1,0:T(4,128)} copy(f32[4,1]{0,1:T(1,128)} %bitcast.10) | data formatting | bytes 32 | tf_op jit(solution)/shard_map/broadcast_in_dim | solution.py:371
  1.9 1.4 %fusion.2.gw = bf16[32,2048]{1,0:T(8,128)(2,1)} fusion(bf16[4,2048]{1,0:T(4,128)(2,1)} %bitcast.8, bf16[4,2048]{1,0:T(4,128)(2,1)} %bitcast.9), kind=kLoop, calls=%fused_computation.3 | loop fusion | flops 458752 | bytes 163840 | tf_op jit(solution)/shard_map/concatenate | solution.py:331
  3.4 54.8 %shard_map.118 = (bf16[8,96,256]{2,1,0:T(8,128)(2,1)}, bf16[8,96,512]{2,1,0:T(8,128)(2,1)}, f32[4,256,128]{2,1,0:T(8,128)}, f32[4,4,64]{2,1,0:T(4,128)}, f32[4,4]{1,0:T(4,128)}, /*index=5*/f32[4,512]{1,0:T(4,128)}) custom-call(bf16[768,2048]{1,0:T(8,128)(2,1)} %bitcast.7, bf16[2048,256]{1,0:T(8,128)(2,1)} %kw.1, bf16[2048,512]{1,0:T(8,128)(2,1)} %vw.1, ...), custom_call_target="tpu_custom_call" | custom-call | tf_op jit(solution)/shard_map/pallas_call | solution.py:337
  58.2 3.7 %shard_map.119 = (bf16[8,96,256]{2,1,0:T(8,128)(2,1)}, bf16[8,96,512]{2,1,0:T(8,128)(2,1)}, f32[4,256,128]{2,1,0:T(8,128)}, f32[4,4,64]{2,1,0:T(4,128)}, f32[4,4]{1,0:T(4,128)}, /*index=5*/f32[4,512]{1,0:T(4,128)}) custom-call(bf16[8,96,256]{2,1,0:T(8,128)(2,1)} %get-tuple-element.18.k_in, bf16[8,96,512]{2,1,0:T(8,128)(2,1)} %get-tuple-element.19.v_in, ...), custom_call_target="tpu_custom_call" | custom-call | tf_op jit(solution)/shard_map/pallas_call | solution.py:372

commit v4 on v3

--- a/solution.py
+++ b/solution.py
@@ -127,17 +127,10 @@
 
     def project(k):
         s = turn(k)
-        load(k).wait()
         block = tokens[pl.ds(pl.multiple_of(s * span, span), span), :]
         keys = jnp.dot(block, key_w[...], preferred_element_type=jnp.float32).astype(jnp.bfloat16)
         for b in range(pieces):
             key_send[s * pieces + b] = keys[b * sub : (b + 1) * sub]
-        gates = lax.dot_general(
-            block, gw[...], (((1,), (1,)), ((), ())), preferred_element_type=jnp.float32
-        ).T
-        fpre = gates[heads : 2 * heads] + bias[...]
-        gate_send[s, 0:heads, :] = gates[0:heads]
-        gate_send[s, heads : 2 * heads, :] = jnp.minimum(fpre, 0.0) - jnp.log1p(jnp.exp(-jnp.abs(fpre)))
         values = jnp.dot(block, val_w[...], preferred_element_type=jnp.float32).astype(jnp.bfloat16)
         for b in range(pieces):
             val_send[s * pieces + b] = values[b * sub : (b + 1) * sub]
@@ -146,19 +139,32 @@
     def step(k, carry):
         s = project(k)
         for b in range(pieces):
-            gate_copy(s * pieces + b).start()
-        for b in range(pieces):
             key_copy(s * pieces + b).start()
             val_copy(s * pieces + b).start()
         return carry
 
     key_load.wait()
     val_load.wait()
-    lax.fori_loop(0, seqs - 1, step, 0)
+    load(0).wait()
+    step(0, 0)
+    for k in range(1, seqs):
+        load(k).wait()
+    gates = lax.dot_general(
+        tokens[...], gw[...], (((1,), (1,)), ((), ())), preferred_element_type=jnp.float32
+    ).T
+    own = lax.broadcasted_iota(jnp.int32, (heads, heads), 0) == lax.broadcasted_iota(jnp.int32, (heads, heads), 1)
+    shift = jnp.sum(jnp.where(own, jnp.broadcast_to(bias[...], (heads, heads)), 0.0), axis=1, keepdims=True)
+    fpre = gates[heads : 2 * heads] + shift
+    logf = jnp.minimum(fpre, 0.0) - jnp.log1p(jnp.exp(-jnp.abs(fpre)))
+    for s in range(seqs):
+        gate_send[s, 0:heads, :] = gates[0:heads, s * span : (s + 1) * span]
+        gate_send[s, heads : 2 * heads, :] = logf[:, s * span : (s + 1) * span]
+    for k in range(1, size):
+        gate_copy((me + k) % size).start()
+    lax.fori_loop(1, seqs - 1, step, 0)
     project(seqs - 1)
     for j in range(1, pieces):
         to = seq * pieces + (piece + j) % pieces
-        gate_copy(to).start()
         key_copy(to).start()
         val_copy(to).start()
     key_out[me] = key_send[me]
@@ -368,7 +374,7 @@
         compiler_params=pltpu.CompilerParams(
             collective_id=0, has_side_effects=True, vmem_limit_bytes=63 * 1024 * 1024
         ),
-    )(tokens.reshape(seqs * span, width), key_weight, value_weight, gates, forget_bias[:, None], query)
+    )(tokens.reshape(seqs * span, width), key_weight, value_weight, gates, forget_bias[None, :], query)
     outs = pl.pallas_call(
         write_out,
         out_shape=tuple(jax.ShapeDtypeStruct(x.shape, x.dtype) for x in outs),

time: 62.3 us -> 60.6 us (0.973)
  local copies, waits for them, and re-layouts: 1.31 us -> 0 us
    broadcast_in_dim x1 -> x0, local copies, waits for them, and re-layouts: 1.31 us -> none  [local(): forget_bias[:, None]]
where the time goes in v4:
time: 60.6 us; the launch traced here: 60.1 us
  Pallas kernels  58.1 us (96%)
  other arithmetic  1.41 us (2%)
  between operations  0.64 us (1%)
    pallas_call x1, Pallas kernels, local(): pl.pallas_call(functools.partial(kernel, (seqs, span, heads, kdim, vdim,...  54.4 us
    pallas_call x1, Pallas kernels, local(): pl.pallas_call(write_out, out_shape=tuple((jax.ShapeDtypeStruct(x.shape,...  3.69 us
    concatenate x1, other arithmetic, local(): gates = jnp.concatenate([input_weight.T, forget_weight.T], axis=0)  1.41 us

profile of v4, /device:TPU:0, one launch (start us, length us, event | category | flops | bytes accessed | tf_op | source)
XLA Modules:
  0.0 60.1 jit_solution(12990325084761903988)
XLA Ops:
  0.6 1.4 %fusion.2.gw = bf16[32,2048]{1,0:T(8,128)(2,1)} fusion(bf16[4,2048]{1,0:T(4,128)(2,1)} %bitcast.8, bf16[4,2048]{1,0:T(4,128)(2,1)} %bitcast.9), kind=kLoop, calls=%fused_computation.3 | loop fusion | flops 458752 | bytes 163840 | tf_op jit(solution)/shard_map/concatenate | solution.py:337
  2.0 54.4 %shard_map.118 = (bf16[8,96,256]{2,1,0:T(8,128)(2,1)}, bf16[8,96,512]{2,1,0:T(8,128)(2,1)}, f32[4,256,128]{2,1,0:T(8,128)}, f32[4,4,64]{2,1,0:T(4,128)}, f32[4,4]{1,0:T(4,128)}, /*index=5*/f32[4,512]{1,0:T(4,128)}) custom-call(bf16[768,2048]{1,0:T(8,128)(2,1)} %bitcast.7, bf16[2048,256]{1,0:T(8,128)(2,1)} %kw.1, bf16[2048,512]{1,0:T(8,128)(2,1)} %vw.1, ...), custom_call_target="tpu_custom_call" | custom-call | tf_op jit(solution)/shard_map/pallas_call | solution.py:343
  56.5 3.7 %shard_map.119 = (bf16[8,96,256]{2,1,0:T(8,128)(2,1)}, bf16[8,96,512]{2,1,0:T(8,128)(2,1)}, f32[4,256,128]{2,1,0:T(8,128)}, f32[4,4,64]{2,1,0:T(4,128)}, f32[4,4]{1,0:T(4,128)}, /*index=5*/f32[4,512]{1,0:T(4,128)}) custom-call(bf16[8,96,256]{2,1,0:T(8,128)(2,1)} %get-tuple-element.18.k_in, bf16[8,96,512]{2,1,0:T(8,128)(2,1)} %get-tuple-element.19.v_in, ...), custom_call_target="tpu_custom_call" | custom-call | tf_op jit(solution)/shard_map/pallas_call | solution.py:378
